TPU v7x, 128 devices: a whole 4x4x4 slice. The times are simulated.
128 devices in a mesh: fs: 32 (over z, y, core), tp: 4 (over x).
Axes of the slice: x: 4, y: 4, z: 4, core: 2. Of those that a mesh axis runs over, the one named last changes fastest.
Arguments:
- tokens: bfloat16 [32768, 2048], P('fs'), may hold values from -6 to 6
- norm_gain: float32 [2048], P('fs'), may hold values from 0.1 to 1.9
- gate_train: float32 [32, 2048, 768], P(None, 'fs', 'tp'), may hold values from -0.125 to 0.125
- up_train: float32 [32, 2048, 768], P(None, 'fs', 'tp'), may hold values from -0.125 to 0.125
- down_train: float32 [32, 768, 2048], P(None, 'fs', 'tp'), may hold values from -0.21875 to 0.21875
- expert_ids: int32 [32768, 2], P('fs'), may hold values from 0 to 31, all different within a row; in each aligned block of 1024 rows (0 to 1023, 1024 to 2047, ...) at most 128 rows name the same one
- route_weights: float32 [32768, 2], P('fs'), may hold values from 0.1 to 1
Outputs:
- gate_serve: bfloat16 [32, 2048, 768], P('fs', None, 'tp')
- up_serve: bfloat16 [32, 2048, 768], P('fs', None, 'tp')
- down_serve: bfloat16 [32, 768, 2048], P('fs', 'tp')
- mixed: bfloat16 [32768, 2048], P('fs', 'tp')
Inputs may be any that keep to these rules, and one draw needn't show every extreme that they name: `expert_ids`: each row names 2 different experts. Within each aligned block of 1024 rows no expert is named more than 128 times, and in every block some expert is named exactly 128 times; every expert is named somewhere.
All inputs are finite; a program needn't handle non-finite values.
Results may differ from a plain program's by a relative error of at most 0.011.
Values may be sent and summed in bfloat16 or wider, within the bound.
A program may use at most 128 MiB of HBM per device.

v0:
```python
import jax
import jax.numpy as jnp
from jax import lax
from jax.sharding import PartitionSpec as P

epsilon = 1e-06


def in_one_piece(arrays, axis, split_dim, concat_dim, along):
    ends, at = ([], 0)
    for a in arrays[:-1]:
        at += a.shape[along]
        ends.append(at)
    both = jnp.concatenate(arrays, axis=along)
    return tuple(
        jnp.split(
            lax.all_to_all(both, axis, split_axis=split_dim, concat_axis=concat_dim, tiled=True),
            ends,
            axis=along,
        )
    )


def on_device(tokens, norm_gain, gate_train, up_train, down_train, expert_ids, route_weights):
    fs_count = lax.axis_size("fs")
    tp_count = lax.axis_size("tp")
    experts = gate_train.shape[0]
    local_experts = experts // fs_count
    gate_cast = (norm_gain[None, :, None] * gate_train).astype(jnp.bfloat16)
    up_cast = (norm_gain[None, :, None] * up_train).astype(jnp.bfloat16)
    gate_serve, up_serve = in_one_piece((gate_cast, up_cast), "fs", 0, 1, 2)
    down_serve = lax.all_to_all(
        lax.all_to_all(
            down_train.astype(jnp.bfloat16), "fs", split_axis=0, concat_axis=1, tiled=True
        ),
        "tp",
        split_axis=1,
        concat_axis=2,
        tiled=True,
    )
    tok_float = tokens.astype(jnp.float32)
    normed = (
        tok_float * lax.rsqrt(jnp.mean(tok_float * tok_float, axis=-1, keepdims=True) + epsilon)
    ).astype(jnp.bfloat16)
    tok_rows, picks = expert_ids.shape
    width = tokens.shape[1]
    capacity = 2 * tok_rows * picks // experts
    flat_ids = expert_ids.reshape(-1)
    onehot = (flat_ids[:, None] == jnp.arange(experts, dtype=jnp.int32)[None, :]).astype(jnp.int32)
    slot_rank = jnp.sum((jnp.cumsum(onehot, axis=0) - onehot) * onehot, axis=1)
    target = (flat_ids * capacity + slot_rank).reshape(tok_rows, picks)
    slot_ids = jnp.arange(experts * capacity, dtype=jnp.int32)
    dispatch = jnp.zeros((experts * capacity, tok_rows), jnp.bfloat16)
    for pick in range(picks):
        dispatch = dispatch + (slot_ids[:, None] == target[None, :, pick]).astype(jnp.bfloat16)
    outgoing = jnp.dot(dispatch, normed, preferred_element_type=jnp.float32).astype(jnp.bfloat16)
    outgoing = outgoing.reshape(experts, capacity, width)
    quarter = capacity // tp_count
    gate_whole, up_whole, down_whole = (
        lax.all_gather(gate_serve, "tp", axis=2, tiled=True),
        lax.all_gather(up_serve, "tp", axis=2, tiled=True),
        lax.all_gather(down_serve, "tp", axis=1, tiled=True),
    )
    share_rows = lax.dynamic_slice_in_dim(outgoing, lax.axis_index("tp") * quarter, quarter, 1)
    routed = lax.all_to_all(share_rows, "fs", split_axis=0, concat_axis=1, tiled=True)
    gate_act = jnp.einsum("erd,edf->erf", routed, gate_whole, preferred_element_type=jnp.float32)
    up_act = jnp.einsum("erd,edf->erf", routed, up_whole, preferred_element_type=jnp.float32)
    hidden = (jax.nn.silu(gate_act) * up_act).astype(jnp.bfloat16)
    row_count = hidden.shape[1]
    block_width = hidden.shape[2] // tp_count
    hidden_blocks = hidden.reshape(local_experts, row_count, tp_count, block_width)
    down_blocks = down_whole.reshape(local_experts, tp_count, block_width, width)
    partial_value = jnp.einsum(
        "erbf,ebfd->erbd", hidden_blocks, down_blocks, preferred_element_type=jnp.float32
    )
    results = jnp.sum(partial_value.astype(jnp.bfloat16).astype(jnp.float32), axis=2).astype(
        jnp.bfloat16
    )
    returned = lax.all_to_all(
        lax.all_to_all(results, "fs", split_axis=1, concat_axis=0, tiled=True),
        "tp",
        split_axis=2,
        concat_axis=1,
        tiled=True,
    )
    returned_flat = returned.reshape(experts * capacity, returned.shape[2])
    shares = route_weights / jnp.sum(route_weights, axis=-1, keepdims=True)
    mixed = jnp.zeros((tok_rows, returned_flat.shape[1]), jnp.float32)
    for pick in range(picks):
        selector = (target[:, pick][:, None] == slot_ids[None, :]).astype(jnp.bfloat16)
        picked = jnp.dot(selector, returned_flat, preferred_element_type=jnp.float32)
        mixed = mixed + shares[:, pick][:, None] * picked
    return (gate_serve, up_serve, down_serve, mixed.astype(jnp.bfloat16))


def solution(mesh):
    return jax.shard_map(
        on_device,
        mesh=mesh,
        in_specs=(
            P("fs", None),
            P("fs"),
            P(None, "fs", "tp"),
            P(None, "fs", "tp"),
            P(None, "fs", "tp"),
            P("fs", None),
            P("fs", None),
        ),
        out_specs=(P("fs", None, "tp"), P("fs", None, "tp"), P("fs", "tp", None), P("fs", "tp")),
        check_vma=False,
    )
```

profile of v0, /device:TPU:1, one launch (start us, length us, event | category | flops | bytes accessed | tf_op | source)
XLA Modules:
  0.0 481.1 jit_solution(9555785108103193418)
XLA Ops:
  7.2 0.0 all-gather.6.cloned.1.call-start
  7.2 2.9 multiply_convert_fusion.2
  10.1 0.6 pad_maximum_fusion
  10.7 32.1 %all_to_all.78 = bf16[32,64,384]{2,1,0:T(8,128)(2,1)S(1)} all-to-all(bf16[32,64,384]{2,1,0:T(8,128)(2,1)S(1)} %pad_maximum_fusion), channel_id=1, replica_groups=mesh['fs'=32,'tp'=4] {'fs'}, dimensions={0} | all-to-all | bytes 3145728 | tf_op jit(solution)/shard_map/all_to_all | solution.py:17
  42.8 0.5 fusion.25
  43.2 0.0 copy-start
  43.3 1.2 copy.74
  44.5 0.0 all-gather.6.cloned.1.call-update
  44.5 2.4 convert_element_type.50
  46.9 4.4 all-to-all-start.1
  51.4 0.0 copy-done
  51.4 0.2 copy.62
  51.6 0.3 eq.85
  51.9 0.3 eq.81
  52.2 9.1 %reduce-window.6 = s32[32,16,128]{2,1,0:T(8,128)S(1)} reduce-window(s32[32,16,128]{2,1,0:T(8,128)S(1)} %fusion.24, s32[]{:T(128)} %constant.11.clone.1), window={size=1x1x128 pad=0_0x0_0x127_0}, to_apply=%region_1.0 | reduce-window | flops 8323072 | bytes 524292 | tf_op jit(solution)/shard_map/reduce-window
  61.2 0.1 slice.27
  61.4 0.2 copy.75
  61.6 0.2 reduce-window.9
  61.8 0.1 broadcast_add_fusion
  62.0 3.1 fusion.4
  65.1 0.1 fusion.23
  65.2 0.5 reduce_sum.45
  65.7 0.2 copy.66
  65.9 0.0 all-to-all-done.1
  65.9 1.2 copy.85
  67.1 0.5 broadcast.36
  67.6 5.4 %reduce.5 = bf16[768,512]{1,0:T(8,128)(2,1)S(1)} reduce(bf16[768,1,512]{2,1,0:T(2,128)(2,1)S(1)} %bitcast.71, bf16[]{:T(256)} %broadcast.36), dimensions={1}, to_apply=%bitcast.62.reduce_sub_computation | reduce | bytes 1572866
  73.1 1.4 reshape.102
  74.4 4.0 all-to-all-start.2
  78.5 10.8 %all-gather.4.cloned.1.call-start = ((), (), s32[]{:S(2)}) async-start(), calls=%async_computation.6 | async-start | bytes 3932160 | tf_op jit(solution)/shard_map/all_gather | solution.py:60
  89.3 1.2 copy.73
  90.5 0.0 all-gather.4.cloned.1.call-update
  90.5 23.5 %convolution_convert_fusion = bf16[4096,2048]{1,0:T(8,128)(2,1)} fusion(s32[1024]{0:T(1024)S(1)} %bitcast.84, s32[1024]{0:T(1024)S(1)} %bitcast.86, bf16[1024,2048]{1,0:T(8,128)(2,1)} %param.7, f32[1024]{0:T(1024)S(1)} %add_rsqrt_fusion), kind=kOutput, calls=%fused_computation.9 | convolution fusion | flops 17228103680 | bytes 20983808 | tf_op jit(solution)/shard_map/dot_general | solution.py:56
  114.1 4.7 constant_dynamic-slice_fusion
  118.8 0.0 all-to-all-done.2
  118.8 7.8 %all-to-all-start.3 = ((bf16[32,32,2048]{2,1,0:T(8,128)(2,1)}), bf16[32,32,2048]{2,1,0:T(8,128)(2,1)}, u32[]{:S(2)}, u32[]{:S(2)}) async-start(bf16[32,32,2048]{2,1,0:T(8,128)(2,1)} %constant_dynamic-slice_fusion), calls=%async_computation.3 | async-start | bytes 8388608 | tf_op jit(solution)/shard_map/all_to_all | solution.py:65
  126.6 0.0 all-gather.8.cloned.1.call-start
  126.7 0.8 reshape.103
  127.4 0.2 copy.77
  127.7 1.0 copy.79
  128.6 0.0 all-gather.8.cloned.1.call-update
  128.7 48.6 %all-to-all-done.3 = bf16[32,32,2048]{2,1,0:T(8,128)(2,1)} async-done(((bf16[32,32,2048]{2,1,0:T(8,128)(2,1)}), bf16[32,32,2048]{2,1,0:T(8,128)(2,1)}, u32[]{:S(2)}, u32[]{:S(2)}) %all-to-all-start.3) | async-done | bytes 4194336 | tf_op jit(solution)/shard_map/all_to_all | solution.py:65
  177.3 0.0 all-gather.6.cloned.1.call-done
  177.3 8.3 %fusion.15 = f32[1024,768]{0,1:T(8,128)} fusion(bf16[1024,2048]{1,0:T(8,128)(2,1)} %bitcast.10, bf16[1,2048,768]{1,2,0:T(8,128)(2,1)} %all-gather.6.cloned.1.call-done), kind=kOutput, calls=%fused_computation.20 | convolution fusion | flops 3221225472 | bytes 10485760 | tf_op jit(solution)/shard_map/erd,edf->erf/dot_general | solution.py:67
  185.6 0.0 all-gather.4.cloned.1.call-done
  185.6 7.9 %multiply_convert_fusion = bf16[1024,768]{0,1:T(8,128)(2,1)S(1)} fusion(f32[1024,768]{0,1:T(8,128)} %fusion.15, bf16[1024,2048]{1,0:T(8,128)(2,1)} %bitcast.10, bf16[1,2048,768]{1,2,0:T(8,128)(2,1)} %all-gather.4.cloned.1.call-done), kind=kOutput, calls=%fused_computation.24 | convolution fusion | flops 3225944064 | bytes 12058624 | tf_op jit(solution)/shard_map/erd,edf->erf/dot_general | solution.py:66
  193.5 0.0 all-gather.8.cloned.1.call-done
  193.5 9.7 %convert_reduce_fusion = bf16[1024,2048]{1,0:T(8,128)(2,1)} fusion(bf16[1024,4,192]{0,2,1:T(8,128)(2,1)S(1)} %bitcast.91, bf16[4,192,2048]{2,1,0:T(8,128)(2,1)} %bitcast.90), kind=kOutput, calls=%fused_computation.1 | convolution fusion | flops 3235905536 | bytes 8912896 | tf_op jit(solution)/shard_map/erbf,ebfd->erbd/dot_general | solution.py:73
  203.2 8.6 %copy.84 = bf16[1,1024,2048]{2,0,1:T(2,128)(2,1)} copy(bf16[1,1024,2048]{2,1,0:T(8,128)(2,1)} %bitcast.73) | data formatting | bytes 8388608 | tf_op jit(solution)/shard_map/reduce_sum | solution.py:76
  211.8 27.1 %reduce.6 = bf16[1024,2048]{1,0:T(8,128)(2,1)} reduce(bf16[1024,1,2048]{2,1,0:T(2,128)(2,1)} %bitcast.66, bf16[]{:T(256)} %broadcast.36), dimensions={1}, to_apply=%bitcast.61.reduce_sub_computation | reduce | bytes 8388610
  238.9 7.8 %reshape.104 = bf16[32,2,32768]{2,1,0:T(2,128)(2,1)} reshape(bf16[1024,2048]{1,0:T(8,128)(2,1)} %reduce.6) | data formatting | bytes 8388608
  246.7 58.9 %all_to_all.79 = bf16[32,2,32768]{2,1,0:T(2,128)(2,1)} all-to-all(bf16[32,2,32768]{2,1,0:T(2,128)(2,1)} %reshape.104), channel_id=1, replica_groups=mesh['fs'=32,'tp'=4] {'fs'}, dimensions={0} | all-to-all | bytes 8388608 | tf_op jit(solution)/shard_map/all_to_all | solution.py:80
  305.7 19.8 %reshape.105 = bf16[1024,1,2048]{2,1,0:T(2,128)(2,1)} reshape(bf16[32,2,32768]{2,1,0:T(2,128)(2,1)} %all_to_all.79) | data formatting | bytes 8388608
  325.4 7.9 %copy.78 = bf16[1,1024,2048]{2,1,0:T(8,128)(2,1)} copy(bf16[1,1024,2048]{2,0,1:T(2,128)(2,1)} %bitcast.67) | data formatting | bytes 8388608
  333.4 23.0 %copy.70 = bf16[32,32,2048]{1,0,2:T(8,128)(2,1)} copy(bf16[32,32,2048]{2,1,0:T(8,128)(2,1)} %bitcast.68) | data formatting | bytes 8388608 | tf_op jit(solution)/shard_map/all_to_all | solution.py:80
  356.4 19.2 %reshape.106 = bf16[4,2,262144]{2,1,0:T(2,128)(2,1)} reshape(bf16[2048,32,32]{2,1,0:T(8,128)(2,1)} %bitcast.64) | data formatting | bytes 8388608
  375.6 5.0 %all-to-all-start.5 = ((bf16[4,2,262144]{2,1,0:T(2,128)(2,1)}), bf16[4,2,262144]{2,1,0:T(2,128)(2,1)}, u32[]{:S(2)}, u32[]{:S(2)}) async-start(bf16[4,2,262144]{2,1,0:T(2,128)(2,1)} %reshape.106), calls=%async_computation.5 | async-start | bytes 8388608 | tf_op jit(solution)/shard_map/all_to_all | solution.py:79
  380.6 0.0 copy-done.1
  380.7 49.1 %all-to-all-done.5 = bf16[4,2,262144]{2,1,0:T(2,128)(2,1)} async-done(((bf16[4,2,262144]{2,1,0:T(2,128)(2,1)}), bf16[4,2,262144]{2,1,0:T(2,128)(2,1)}, u32[]{:S(2)}, u32[]{:S(2)}) %all-to-all-start.5) | async-done | bytes 4194336 | tf_op jit(solution)/shard_map/all_to_all | solution.py:79
  429.8 12.0 %reshape.107 = bf16[2048,32,32]{2,1,0:T(8,128)(2,1)} reshape(bf16[4,2,262144]{2,1,0:T(2,128)(2,1)} %all-to-all-done.5) | data formatting | bytes 8388608
  441.8 19.0 %copy.76 = bf16[32,32,4,512]{3,2,1,0:T(4,128)(2,1)} copy(bf16[32,32,4,512]{1,0,3,2:T(8,128)(2,1)} %bitcast.65) | data formatting | bytes 8388608 | tf_op jit(solution)/shard_map/all_to_all | solution.py:79
  460.8 3.5 copy.72
  464.3 4.5 fusion
  468.8 5.6 %add_convert_fusion = bf16[1024,512]{1,0:T(8,128)(2,1)} fusion(f32[1024,512]{1,0:T(8,128)S(1)} %fusion, bf16[4096,512]{1,0:T(8,128)(2,1)S(1)} %bitcast.75, s32[1024]{0:T(1024)S(1)} %bitcast.85, f32[1024]{0:T(1024)S(1)} %bitcast.89, f32[1024]{0:T(1024)S(1)} %bitcast.88), kind=kOutput, calls=%fused_computation.25 | convolution fusion | flops 4301258752 | bytes 7352320 | tf_op jit(solution)/shard_map/dot_general | solution.py:91
  (8 shorter events, 0.1 us)
Async XLA Ops:
  7.2 170.1 %all-gather.6.cloned.1.call-start = ((), (), s32[]{:S(2)}) async-start(), calls=%async_computation.7 | async-start | bytes 3932160 | tf_op jit(solution)/shard_map/all_gather | solution.py:61
  43.2 8.1 %copy-start = (s32[1024,2]{0,1:T(2,128)S(1)}, s32[1024,2]{0,1:T(2,128)}, u32[]{:S(2)}) copy-start(s32[1024,2]{0,1:T(2,128)} %param.12) | copy-start | bytes 24580
  46.9 19.0 %all-to-all-start.1 = ((bf16[32,24,512]{2,1,0:T(8,128)(2,1)}), bf16[32,24,512]{2,1,0:T(8,128)(2,1)S(1)}, u32[]{:S(2)}, u32[]{:S(2)}) async-start(bf16[32,24,512]{2,1,0:T(8,128)(2,1)} %convert_element_type.50), calls=%async_computation.1 | async-start | bytes 1572864 | tf_op jit(solution)/shard_map/all_to_all | solution.py:33
  74.4 44.3 %all-to-all-start.2 = ((bf16[4,2,49152]{2,1,0:T(2,128)(2,1)}), bf16[4,2,49152]{2,1,0:T(2,128)(2,1)S(1)}, u32[]{:S(2)}, u32[]{:S(2)}) async-start(bf16[4,2,49152]{2,1,0:T(2,128)(2,1)} %reshape.102), calls=%async_computation.2 | async-start | bytes 1572864 | tf_op jit(solution)/shard_map/all_to_all | solution.py:32
  78.5 107.2 %all-gather.4.cloned.1.call-start = ((), (), s32[]{:S(2)}) async-start(), calls=%async_computation.6 | async-start | bytes 3932160 | tf_op jit(solution)/shard_map/all_gather | solution.py:60
  118.8 58.5 %all-to-all-start.3 = ((bf16[32,32,2048]{2,1,0:T(8,128)(2,1)}), bf16[32,32,2048]{2,1,0:T(8,128)(2,1)}, u32[]{:S(2)}, u32[]{:S(2)}) async-start(bf16[32,32,2048]{2,1,0:T(8,128)(2,1)} %constant_dynamic-slice_fusion), calls=%async_computation.3 | async-start | bytes 8388608 | tf_op jit(solution)/shard_map/all_to_all | solution.py:65
  126.6 66.9 %all-gather.8.cloned.1.call-start = ((), (), s32[]{:S(2)}) async-start(), calls=%async_computation.8 | async-start | bytes 3932160 | tf_op jit(solution)/shard_map/all_gather | solution.py:62
  375.6 5.0 %copy-start.1 = (f32[1024,2]{0,1:T(2,128)S(1)}, f32[1024,2]{0,1:T(2,128)}, u32[]{:S(2)}) copy-start(f32[1024,2]{0,1:T(2,128)} %param.13) | copy-start | bytes 24580
  375.6 54.1 %all-to-all-start.5 = ((bf16[4,2,262144]{2,1,0:T(2,128)(2,1)}), bf16[4,2,262144]{2,1,0:T(2,128)(2,1)}, u32[]{:S(2)}, u32[]{:S(2)}) async-start(bf16[4,2,262144]{2,1,0:T(2,128)(2,1)} %reshape.106), calls=%async_computation.5 | async-start | bytes 8388608 | tf_op jit(solution)/shard_map/all_to_all | solution.py:79
Sparse Core Ops, SparseCore 0:
  44.6 36.8 all-gather.5
  90.7 41.1 all-gather.3
  134.1 39.6 all-gather.7
where the time goes:
time: 481 us
  local copies, waits for them, and re-layouts  135 us (28%)
  waiting for transfers between devices  97.8 us (20%)
  blocking collectives  91 us (19%)
  matrix products  59.5 us (12%)
  other arithmetic  51.1 us (11%)
  starting transfers between devices  32.2 us (7%)
  between operations  14.2 us (3%)
    unnamed x16, local copies, waits for them, and re-layouts  72.3 us
    all_to_all x1, blocking collectives, on_device(): lax.all_to_all(results, 'fs', split_axis=1, concat_axis=0, tiled=True)  58.9 us
    all_to_all x1, waiting for transfers between devices, on_device(): lax.all_to_all(lax.all_to_all(results, 'fs', split_axis=1, concat_axis=0,...  49.1 us
    all_to_all x1, waiting for transfers between devices, on_device(): lax.all_to_all(share_rows, 'fs', split_axis=0, concat_axis=1, tiled=True)  48.6 us
    unnamed x2, other arithmetic  32.5 us
    all_to_all x1, blocking collectives, in_one_piece(): lax.all_to_all(both, axis, split_axis=split_dim, concat_axis=concat_dim,...  32.1 us
    dot_general x1, matrix products, on_device(): jnp.dot(dispatch, normed, preferred_element_type=jnp.float32)  23.5 us
    all_to_all x1, local copies, waits for them, and re-layouts, on_device(): lax.all_to_all(results, 'fs', split_axis=1, concat_axis=0, tiled=True)  23 us
  transfers between devices with their start and end apart: 7, of which 2 were waited for; matrix products, arithmetic and copies ran while one was open for 15% of the time, Pallas kernels for 0%

commit v1 on v0

v1 whole, which is shorter than its diff:
```python
import jax
import jax.numpy as jnp
from jax import lax
from jax.sharding import PartitionSpec as P

epsilon = 1e-06


def on_device(tokens, norm_gain, gate_train, up_train, down_train, expert_ids, route_weights):
    fs_count = lax.axis_size("fs")
    tp_count = lax.axis_size("tp")
    my_tp = lax.axis_index("tp")
    experts, rows_gate, cols_gate = gate_train.shape
    rows_down, cols_down = down_train.shape[1:]
    tok_rows, picks = expert_ids.shape
    width = tokens.shape[1]
    capacity = 2 * tok_rows * picks // experts
    quarter = capacity // tp_count
    bf16, f32 = jnp.bfloat16, jnp.float32

    gate_cast = (norm_gain[None, :, None] * gate_train).astype(bf16)
    up_cast = (norm_gain[None, :, None] * up_train).astype(bf16)
    both = lax.all_to_all(
        jnp.concatenate([gate_cast, up_cast], axis=2), "fs", split_axis=0, concat_axis=0, tiled=True
    ).reshape(1, fs_count * rows_gate, 2 * cols_gate)
    gate_serve, up_serve = both[:, :, :cols_gate], both[:, :, cols_gate:]
    down_rows = lax.all_to_all(
        down_train.astype(bf16), "fs", split_axis=0, concat_axis=0, tiled=True
    ).reshape(tp_count, fs_count * rows_down // tp_count, cols_down)
    down_cols = lax.all_to_all(down_rows, "tp", split_axis=0, concat_axis=0, tiled=True)
    down_serve = jnp.swapaxes(down_cols, 0, 1).reshape(1, down_rows.shape[1], width)
    gate_whole, up_whole, down_whole = (
        lax.all_gather(gate_serve[0], "tp", axis=1, tiled=True),
        lax.all_gather(up_serve[0], "tp", axis=1, tiled=True),
        lax.all_gather(down_serve[0], "tp", axis=0, tiled=True),
    )

    tok_float = tokens.astype(f32)
    normed = (
        tok_float * lax.rsqrt(jnp.mean(tok_float * tok_float, axis=-1, keepdims=True) + epsilon)
    ).astype(bf16)
    lane = jnp.arange(experts, dtype=jnp.int32)[None, :]
    hot = [expert_ids[:, k][:, None] == lane for k in range(picks)]
    named = sum(h.astype(bf16) for h in hot)
    at = jnp.arange(tok_rows, dtype=jnp.int32)
    before = jnp.dot((at[None, :] < at[:, None]).astype(bf16), named, preferred_element_type=f32)
    slot = [jnp.sum(jnp.where(h, before, 0.0), axis=1).astype(jnp.int32) for h in hot]
    target = [expert_ids[:, k] * capacity + slot[k] for k in range(picks)]

    mine = jnp.arange(experts * quarter, dtype=jnp.int32)
    mine = (mine // quarter) * capacity + my_tp * quarter + mine % quarter
    dispatch = sum((mine[:, None] == t[None, :]).astype(bf16) for t in target)
    outgoing = jnp.dot(dispatch, normed, preferred_element_type=f32).astype(bf16)
    routed = lax.all_to_all(
        outgoing.reshape(experts, quarter, width), "fs", split_axis=0, concat_axis=0, tiled=True
    ).reshape(fs_count * quarter, width)

    gate_act = jnp.dot(routed, gate_whole, preferred_element_type=f32)
    up_act = jnp.dot(routed, up_whole, preferred_element_type=f32)
    hidden = (jax.nn.silu(gate_act) * up_act).astype(bf16)
    results = jnp.dot(hidden, down_whole, preferred_element_type=f32).astype(bf16)
    results = results.reshape(fs_count, quarter, tp_count, width // tp_count)
    results = jnp.swapaxes(results, 1, 2).reshape(fs_count * tp_count, quarter, width // tp_count)
    returned = lax.all_to_all(results, ("fs", "tp"), split_axis=0, concat_axis=0, tiled=True)
    returned = returned.reshape(experts * capacity, width // tp_count)

    slot_ids = jnp.arange(experts * capacity, dtype=jnp.int32)
    total = jnp.sum(route_weights, axis=-1)
    mixed = 0.0
    for k in range(picks):
        selector = (target[k][:, None] == slot_ids[None, :]).astype(bf16)
        picked = jnp.dot(selector, returned, preferred_element_type=f32)
        mixed = mixed + (route_weights[:, k] / total)[:, None] * picked
    return (gate_serve, up_serve, down_serve, mixed.astype(bf16))


def solution(mesh):
    return jax.shard_map(
        on_device,
        mesh=mesh,
        in_specs=(
            P("fs", None),
            P("fs"),
            P(None, "fs", "tp"),
            P(None, "fs", "tp"),
            P(None, "fs", "tp"),
            P("fs", None),
            P("fs", None),
        ),
        out_specs=(P("fs", None, "tp"), P("fs", None, "tp"), P("fs", "tp", None), P("fs", "tp")),
        check_vma=False,
    )
```

time: 481 us -> 285 us (0.59)
  local copies, waits for them, and re-layouts: 135 us -> 19.3 us
  other arithmetic: 51.1 us -> 8.43 us
  starting transfers between devices: 32.2 us -> 15.6 us
  blocking collectives: 91 us -> 74.5 us
  matrix products: 59.5 us -> 43.6 us
  waiting for transfers between devices: 97.8 us -> 109 us
    unnamed x16 -> x8, local copies, waits for them, and re-layouts: 72.3 us -> 2.49 us
    all_to_all x5 -> x0, local copies, waits for them, and re-layouts: 47.7 us -> none  [the longest x1 23 us: on_device(): lax.all_to_all(results, 'fs', split_axis=1, concat_axis=0, tiled=True)]
    unnamed x2 -> x0, other arithmetic: 32.5 us -> none
    all_to_all x2 -> x3, blocking collectives: 91 us -> 74.5 us  [the longest x1 32.1 us: on_device(): lax.all_to_all(jnp.concatenate([gate_cast, up_cast], axis=2), 'fs', split...]
    dot_general x6, matrix products: 59.5 us -> 43.6 us  [the longest x2 15.1 us: on_device(): picked = jnp.dot(selector, returned, preferred_element_type=f32)]
    reshape x0 -> x3, local copies, waits for them, and re-layouts: none -> 14.7 us  [the longest x2 13.3 us: on_device(): results = results.reshape(fs_count, quarter, tp_count, width // tp_count)]
    all_gather x3, starting transfers between devices: 10.9 us -> 0.3 us  [the longest x1 0.22 us: on_device(): lax.all_gather(gate_serve[0], 'tp', axis=1, tiled=True)]
    another operation x3 -> x0, other arithmetic: 9.41 us -> none
  transfers between devices with their start and end apart: 7 -> 5, of which waited for: 2 -> 3; matrix products, arithmetic and copies ran while one was open for 15% -> 9% of each run, Pallas kernels for 0% -> 0%
where the time goes in v1:
time: 285 us; the launch traced here: 284 us
  waiting for transfers between devices  109 us (38%)
  blocking collectives  74.5 us (26%)
  matrix products  43.6 us (15%)
  local copies, waits for them, and re-layouts  19.3 us (7%)
  starting transfers between devices  15.6 us (5%)
  between operations  13.9 us (5%)
  other arithmetic  8.43 us (3%)
    all_to_all x1, waiting for transfers between devices, on_device(): lax.all_to_all(results, ('fs', 'tp'), split_axis=0, concat_axis=0, tiled=...  50.8 us
    all_to_all x1, waiting for transfers between devices, on_device(): lax.all_to_all(outgoing.reshape(experts, quarter, width), 'fs', split_axi...  49.2 us
    all_to_all x1, blocking collectives, on_device(): lax.all_to_all(jnp.concatenate([gate_cast, up_cast], axis=2), 'fs', split...  32.1 us
    all_to_all x1, blocking collectives, on_device(): lax.all_to_all(down_rows, 'tp', split_axis=0, concat_axis=0, tiled=True)  24.6 us
    all_to_all x1, blocking collectives, on_device(): lax.all_to_all(down_train.astype(bf16), 'fs', split_axis=0, concat_axis=0...  17.9 us
    dot_general x2, matrix products, on_device(): picked = jnp.dot(selector, returned, preferred_element_type=f32)  15.1 us
    reshape x2, local copies, waits for them, and re-layouts, on_device(): results = results.reshape(fs_count, quarter, tp_count, width // tp_count)  13.3 us
    dot_general x1, matrix products, on_device(): jnp.dot(hidden, down_whole, preferred_element_type=f32).astype(bf16)  13.3 us
  transfers between devices with their start and end apart: 5, of which 3 were waited for; matrix products, arithmetic and copies ran while one was open for 9% of the time, Pallas kernels for 0%

profile of v1, /device:TPU:1, one launch (start us, length us, event | category | flops | bytes accessed | tf_op | source)
XLA Modules:
  0.0 284.0 jit_solution(990886523276557550)
XLA Ops:
  7.2 0.0 all-gather.10.cloned.1.call-start
  7.2 2.9 %multiply_convert_fusion.2 = (bf16[32,64,192]{2,1,0:T(8,128)(2,1)S(1)}, bf16[32,64,192]{2,1,0:T(8,128)(2,1)S(1)}) fusion(f32[32,64,192]{2,1,0:T(8,128)} %param.9, f32[64]{0:T(128)} %param.8, f32[32,64,192]{2,1,0:T(8,128)} %param.10), kind=kLoop, calls=%fused_computation.28 | loop fusion | flops 1572864 | bytes 4718848 | tf_op jit(solution)/shard_map/convert_element_type | solution.py:21
  10.1 0.6 pad_maximum_fusion
  10.7 32.1 %all_to_all.25 = bf16[32,64,384]{2,1,0:T(8,128)(2,1)S(1)} all-to-all(bf16[32,64,384]{2,1,0:T(8,128)(2,1)S(1)} %pad_maximum_fusion), channel_id=1, replica_groups=mesh['fs'=32,'tp'=4] {'fs'}, dimensions={0} | all-to-all | bytes 3145728 | tf_op jit(solution)/shard_map/all_to_all | solution.py:23
  42.8 0.5 fusion.44
  43.2 1.2 copy.28
  44.5 0.0 all-gather.10.cloned.1.call-update
  44.5 0.0 all-gather.6.cloned.1.call-start
  44.5 1.5 convert_element_type.78
  46.1 0.0 copy-start.1
  46.1 17.9 %all_to_all.26 = bf16[32,24,512]{2,1,0:T(8,128)(2,1)S(1)} all-to-all(bf16[32,24,512]{2,1,0:T(8,128)(2,1)S(1)} %convert_element_type.78), channel_id=1, replica_groups=mesh['fs'=32,'tp'=4] {'fs'}, dimensions={0} | all-to-all | bytes 1572864 | tf_op jit(solution)/shard_map/all_to_all | solution.py:27
  63.9 24.6 %all_to_all.27 = bf16[4,192,512]{2,1,0:T(8,128)(2,1)S(1)} all-to-all(bf16[4,192,512]{2,1,0:T(8,128)(2,1)S(1)} %bitcast.41), channel_id=1, replica_groups=mesh['fs'=32,'tp'=4] {'tp'}, dimensions={0} | all-to-all | bytes 1572864 | tf_op jit(solution)/shard_map/all_to_all | solution.py:30
  88.5 1.0 copy.29
  89.5 0.0 all-gather.6.cloned.1.call-update
  89.5 0.0 copy-start
  89.5 0.0 copy-done.1
  89.6 0.5 select_reduce_fusion.1
  90.1 3.4 %fusion.2 = f32[1024]{0:T(1024)S(1)} fusion(bf16[1024,2048]{1,0:T(8,128)(2,1)} %param.7), kind=kLoop, calls=%fused_computation.6 | loop fusion | flops 6290432 | bytes 4198400 | tf_op jit(solution)/shard_map/reduce_sum | solution.py:40
  93.5 0.0 copy-done
  93.5 6.4 %fusion.10 = bf16[1024,2048]{1,0:T(8,128)(2,1)} fusion(bf16[1024,2048]{1,0:T(8,128)(2,1)S(1)} %copy-done, f32[1024]{0:T(1024)S(1)} %add_rsqrt_fusion, s32[1024]{0:T(1024)S(1)} %get-tuple-element.28, s32[1024]{0:T(1024)S(1)} %get-tuple-element.29, s32[1024]{0:T(1024)S(1)} %fusion.41), kind=kOutput, calls=%fused_computation.16 | convolution fusion | flops 4308598784 | bytes 8404992 | tf_op jit(solution)/shard_map/dot_general | solution.py:53
  99.9 6.2 %all-to-all-start.3 = ((bf16[32,32,2048]{2,1,0:T(8,128)(2,1)}), bf16[32,32,2048]{2,1,0:T(8,128)(2,1)}, u32[]{:S(2)}, u32[]{:S(2)}) async-start(bf16[32,32,2048]{2,1,0:T(8,128)(2,1)} %bitcast.39), calls=%async_computation.3 | async-start | bytes 8388608 | tf_op jit(solution)/shard_map/all_to_all | solution.py:54
  106.1 0.2 all-gather.8.cloned.1.call-start
  106.3 1.2 copy.27
  107.6 0.0 all-gather.8.cloned.1.call-update
  107.6 49.2 %all-to-all-done.3 = bf16[32,32,2048]{2,1,0:T(8,128)(2,1)} async-done(((bf16[32,32,2048]{2,1,0:T(8,128)(2,1)}), bf16[32,32,2048]{2,1,0:T(8,128)(2,1)}, u32[]{:S(2)}, u32[]{:S(2)}) %all-to-all-start.3) | async-done | bytes 4194336 | tf_op jit(solution)/shard_map/all_to_all | solution.py:54
  156.8 0.0 all-gather.10.cloned.1.call-done
  156.8 8.3 %fusion.13 = f32[1024,768]{1,0:T(8,128)} fusion(bf16[1024,2048]{1,0:T(8,128)(2,1)} %bitcast.10, bf16[1,2048,768]{1,2,0:T(8,128)(2,1)} %all-gather.10.cloned.1.call-done), kind=kOutput, calls=%fused_computation.18 | convolution fusion | flops 3221225472 | bytes 10485760 | tf_op jit(solution)/shard_map/dot_general | solution.py:59
  165.1 0.0 all-gather.6.cloned.1.call-done
  165.1 8.6 %all-gather.8.cloned.1.call-done = bf16[1,2048,768]{1,2,0:T(8,128)(2,1)} async-done(((bf16[1,2048,192]{1,2,0:T(8,128)(2,1)}), bf16[1,2048,768]{1,2,0:T(8,128)(2,1)}) %all-gather.8.cloned.1.call-update) | async-done | bytes 3145744 | tf_op jit(solution)/shard_map/all_gather | solution.py:33
  173.7 13.3 %convolution_convert_fusion = bf16[1024,2048]{1,0:T(8,128)(2,1)} fusion(bf16[768,2048]{1,0:T(8,128)(2,1)} %all-gather.6.cloned.1.call-done, f32[1024,768]{1,0:T(8,128)} %fusion.13, bf16[1024,2048]{1,0:T(8,128)(2,1)} %bitcast.10, bf16[1,2048,768]{1,2,0:T(8,128)(2,1)} %all-gather.8.cloned.1.call-done), kind=kOutput, calls=%fused_computation.17 | convolution fusion | flops 6449266688 | bytes 17825792 | tf_op jit(solution)/shard_map/dot_general | solution.py:61
  187.0 7.8 %reshape.105 = bf16[32,32,4,512]{3,2,1,0:T(4,128)(2,1)} reshape(bf16[1024,2048]{1,0:T(8,128)(2,1)} %convolution_convert_fusion) | data formatting | bytes 8388608 | tf_op jit(solution)/shard_map/reshape | solution.py:62
  194.8 5.5 %copy.26 = bf16[32,32,4,512]{3,1,2,0:T(8,128)(2,1)} copy(bf16[32,32,4,512]{3,2,1,0:T(4,128)(2,1)} %reshape.105) | data formatting | bytes 8388608 | tf_op jit(solution)/shard_map/reshape | solution.py:62
  200.2 0.0 copy-start.2
  200.2 9.1 %all-to-all-start.4 = ((bf16[128,32,512]{2,1,0:T(8,128)(2,1)}), bf16[128,32,512]{2,1,0:T(8,128)(2,1)}, u32[]{:S(2)}, u32[]{:S(2)}) async-start(bf16[128,32,512]{2,1,0:T(8,128)(2,1)} %bitcast.35), calls=%async_computation.4 | async-start | bytes 8388608 | tf_op jit(solution)/shard_map/all_to_all | solution.py:64
  209.4 0.0 copy-done.2
  209.5 0.6 copy.22
  210.1 1.5 reshape.102
  211.6 50.8 %all-to-all-done.4 = bf16[128,32,512]{2,1,0:T(8,128)(2,1)} async-done(((bf16[128,32,512]{2,1,0:T(8,128)(2,1)}), bf16[128,32,512]{2,1,0:T(8,128)(2,1)}, u32[]{:S(2)}, u32[]{:S(2)}) %all-to-all-start.4) | async-done | bytes 4194336 | tf_op jit(solution)/shard_map/all_to_all | solution.py:64
  262.4 7.3 %fusion = f32[1024,512]{1,0:T(8,128)S(1)} fusion(bf16[4096,512]{1,0:T(8,128)(2,1)} %bitcast.15, s32[1024]{0:T(1024)S(1)} %bitcast.52), kind=kOutput, calls=%fused_computation.2 | convolution fusion | flops 4299161600 | bytes 6295552 | tf_op jit(solution)/shard_map/dot_general | solution.py:72
  269.7 7.8 %add_convert_fusion = bf16[1024,512]{1,0:T(8,128)(2,1)} fusion(f32[1024,512]{1,0:T(8,128)S(1)} %fusion, bf16[4096,512]{1,0:T(8,128)(2,1)} %bitcast.15, s32[1024]{0:T(1024)S(1)} %bitcast.51, f32[1024]{0:T(1024)S(1)} %bitcast.50, f32[1024]{0:T(1024)S(1)} %bitcast.49), kind=kOutput, calls=%fused_computation.24 | convolution fusion | flops 4301258752 | bytes 7352320 | tf_op jit(solution)/shard_map/dot_general | solution.py:72
  (9 shorter events, 0.1 us)
Async XLA Ops:
  7.2 149.6 %all-gather.10.cloned.1.call-start = ((), (), s32[]{:S(2)}) async-start(), calls=%async_computation.7 | async-start | bytes 3932160 | tf_op jit(solution)/shard_map/all_gather | solution.py:34
  44.5 120.6 %all-gather.6.cloned.1.call-start = ((), (), s32[]{:S(2)}) async-start(), calls=%async_computation.5 | async-start | bytes 3932160 | tf_op jit(solution)/shard_map/all_gather | solution.py:35
  46.1 43.5 %copy-start.1 = (s32[1024,2]{0,1:T(2,128)S(1)}, s32[1024,2]{0,1:T(2,128)}, u32[]{:S(2)}) copy-start(s32[1024,2]{0,1:T(2,128)} %param.12) | copy-start | bytes 24580
  89.5 4.0 %copy-start = (bf16[1024,2048]{1,0:T(8,128)(2,1)S(1)}, bf16[1024,2048]{1,0:T(8,128)(2,1)}, u32[]{:S(2)}) copy-start(bf16[1024,2048]{1,0:T(8,128)(2,1)} %param.7) | copy-start | bytes 12582916
  99.9 56.9 %all-to-all-start.3 = ((bf16[32,32,2048]{2,1,0:T(8,128)(2,1)}), bf16[32,32,2048]{2,1,0:T(8,128)(2,1)}, u32[]{:S(2)}, u32[]{:S(2)}) async-start(bf16[32,32,2048]{2,1,0:T(8,128)(2,1)} %bitcast.39), calls=%async_computation.3 | async-start | bytes 8388608 | tf_op jit(solution)/shard_map/all_to_all | solution.py:54
  106.1 67.6 %all-gather.8.cloned.1.call-start = ((), (), s32[]{:S(2)}) async-start(), calls=%async_computation.6 | async-start | bytes 3932160 | tf_op jit(solution)/shard_map/all_gather | solution.py:33
  200.2 9.2 %copy-start.2 = (f32[1024,2]{0,1:T(2,128)S(1)}, f32[1024,2]{0,1:T(2,128)}, u32[]{:S(2)}) copy-start(f32[1024,2]{0,1:T(2,128)} %param.13) | copy-start | bytes 24580
  200.2 62.1 %all-to-all-start.4 = ((bf16[128,32,512]{2,1,0:T(8,128)(2,1)}), bf16[128,32,512]{2,1,0:T(8,128)(2,1)}, u32[]{:S(2)}, u32[]{:S(2)}) async-start(bf16[128,32,512]{2,1,0:T(8,128)(2,1)} %bitcast.35), calls=%async_computation.4 | async-start | bytes 8388608 | tf_op jit(solution)/shard_map/all_to_all | solution.py:64
Sparse Core Ops, SparseCore 0:
  44.6 45.0 all-gather.9
  91.9 39.7 all-gather.5
  134.0 39.6 all-gather.7
